TPU v7x, 32 devices: a whole 2x2x4 slice. The times are simulated.
32 devices in a mesh: fs: 8 (over z, y), tp: 4 (over x, core).
Axes of the slice: x: 2, y: 2, z: 4, core: 2. Of those that a mesh axis runs over, the one named last changes fastest.
Arguments:
- tokens: bfloat16 [8192, 2048], P('fs', 'tp'), may hold values from -6 to 6
- norm_gain: float32 [2048], P('fs'), may hold values from 0.1 to 1.9
- up_master: float32 [2048, 4096], P('fs', 'tp'), may hold values from -0.125 to 0.125
- down_master: float32 [4096, 2048], P('fs', 'tp'), may hold values from -0.09375 to 0.09375
Outputs:
- mixed: bfloat16 [8192, 2048], P('fs', 'tp')
- up_ready: bfloat16 [2048, 4096], P(None, 'tp')
- down_ready: bfloat16 [4096, 2048], P('tp')
All inputs are finite; a program needn't handle non-finite values.
Results may differ from a plain program's by a relative error of at most 0.0095.
Values may be sent and summed in bfloat16 or wider, within the bound.
A program may use at most 128 MiB of HBM per device.

v0:
```python
import jax
import jax.numpy as jnp
from jax import lax
from jax.sharding import PartitionSpec as P


def shards(tokens, norm_gain, up_master, down_master):
    up_local = (norm_gain[:, None] * up_master).astype(jnp.bfloat16)
    up_ready = lax.all_gather(up_local, "fs", axis=0, tiled=True)
    down_local = down_master.astype(jnp.bfloat16)
    gathered = lax.all_gather(down_local, "fs", axis=0, tiled=True)
    down_ready = lax.all_to_all(gathered, "tp", split_axis=0, concat_axis=1, tiled=True)
    features = lax.all_gather(tokens, "tp", axis=1, tiled=True)
    values = features.astype(jnp.float32)
    mean_square = jnp.mean(values * values, axis=-1, keepdims=True)
    normed = (values * lax.rsqrt(mean_square + 1e-06)).astype(jnp.bfloat16)
    before = jnp.dot(normed, up_ready, preferred_element_type=jnp.float32)
    hidden = jnp.square(jax.nn.relu(before)).astype(jnp.bfloat16)
    partial_value = jnp.dot(hidden, down_ready, preferred_element_type=jnp.float32)
    mixed = lax.psum_scatter(
        partial_value.astype(jnp.bfloat16), "tp", scatter_dimension=1, tiled=True
    )
    return (mixed, up_ready, down_ready)


def solution(mesh):
    return jax.shard_map(
        shards,
        mesh=mesh,
        in_specs=(P("fs", "tp"), P("fs"), P("fs", "tp"), P("fs", "tp")),
        out_specs=(P("fs", "tp"), P(None, "tp"), P("tp", None)),
        check_vma=False,
    )
```

profile of v0, /device:TPU:0, one launch (start us, length us, event | category | flops | bytes accessed | tf_op | source)
XLA Modules:
  0.0 287.9 jit_solution(17428654618168584598)
XLA Ops:
  7.2 0.0 all-gather.8.cloned.1.call-start
  7.2 2.1 convert_element_type.22
  9.3 0.0 all-gather.8.cloned.1.call-update
  9.3 0.0 all-gather.4.cloned.1.call-start
  9.4 0.7 all-gather.4.cloned.1.call-update
  10.1 0.0 all-gather.6.cloned.1.call-start
  10.1 2.1 multiply_convert_fusion.2
  12.3 0.0 all-gather.6.cloned.1.call-update
  12.3 73.9 %all-gather.8.cloned.1.call-done = bf16[4096,512]{1,0:T(8,128)(2,1)} async-done(((bf16[512,512]{1,0:T(8,128)(2,1)}), bf16[4096,512]{1,0:T(8,128)(2,1)}) %all-gather.8.cloned.1.call-update) | async-done | bytes 4194320 | tf_op jit(solution)/shard_map/all_gather | solution.py:11
  86.2 4.9 %all-to-all-start = ((bf16[4,1024,512]{2,1,0:T(8,128)(2,1)}), bf16[4,1024,512]{2,1,0:T(8,128)(2,1)}, u32[]{:S(2)}, u32[]{:S(2)}) async-start(bf16[4,1024,512]{2,1,0:T(8,128)(2,1)} %bitcast.8), calls=%async_computation | async-start | bytes 8388608 | tf_op jit(solution)/shard_map/all_to_all | solution.py:12
  91.1 0.0 reduce-scatter.2.cloned.1.call-start
  91.2 52.2 %all-gather.4.cloned.1.call-done = bf16[1024,2048]{1,0:T(8,128)(2,1)} async-done(((bf16[1024,512]{1,0:T(8,128)(2,1)}), bf16[1024,2048]{1,0:T(8,128)(2,1)}) %all-gather.4.cloned.1.call-update) | async-done | bytes 4194320 | tf_op jit(solution)/shard_map/all_gather | solution.py:13
  143.4 3.1 %fusion = f32[1024]{0:T(1024)S(1)} fusion(bf16[1024,2048]{1,0:T(8,128)(2,1)} %all-gather.4.cloned.1.call-done), kind=kLoop, calls=%fused_computation.2 | loop fusion | flops 6290432 | bytes 4198400 | tf_op jit(solution)/shard_map/reduce_sum | solution.py:15
  146.5 15.3 %all-to-all-done = bf16[4,1024,512]{2,1,0:T(8,128)(2,1)} async-done(((bf16[4,1024,512]{2,1,0:T(8,128)(2,1)}), bf16[4,1024,512]{2,1,0:T(8,128)(2,1)}, u32[]{:S(2)}, u32[]{:S(2)}) %all-to-all-start) | async-done | bytes 4194336 | tf_op jit(solution)/shard_map/all_to_all | solution.py:12
  161.8 6.2 %copy.8 = bf16[4,1024,512]{1,2,0:T(8,128)(2,1)} copy(bf16[4,1024,512]{2,1,0:T(8,128)(2,1)} %all-to-all-done) | data formatting | bytes 8388608 | tf_op jit(solution)/shard_map/all_to_all | solution.py:12
  168.0 50.9 %all-gather.6.cloned.1.call-done = bf16[2048,1024]{1,0:T(8,128)(2,1)} async-done(((bf16[256,1024]{1,0:T(8,128)(2,1)}), bf16[2048,1024]{1,0:T(8,128)(2,1)}) %all-gather.6.cloned.1.call-update) | async-done | bytes 4194320 | tf_op jit(solution)/shard_map/all_gather | solution.py:9
  218.9 14.7 %convolution_convert_fusion = bf16[1024,2048]{1,0:T(8,128)(2,1)} fusion(bf16[1024,2048]{0,1:T(8,128)(2,1)} %bitcast.6, bf16[2048,1024]{1,0:T(8,128)(2,1)} %all-gather.6.cloned.1.call-done, bf16[1024,2048]{1,0:T(8,128)(2,1)} %all-gather.4.cloned.1.call-done, f32[1024]{0:T(1024)S(1)} %add_rsqrt_fusion), kind=kOutput, calls=%fused_computation.7 | convolution fusion | flops 8601468928 | bytes 16781312 | tf_op jit(solution)/shard_map/dot_general | solution.py:19
  233.6 0.0 reduce-scatter.2.cloned.1.call-update
  233.6 6.5 %copy.9 = bf16[1024,2048]{1,0:T(8,128)(2,1)} copy(bf16[1024,2048]{0,1:T(8,128)(2,1)} %bitcast.7) | data formatting | bytes 8388608
  240.1 36.6 %reduce-scatter.2.cloned.1.call-done = bf16[1024,512]{1,0:T(8,128)(2,1)} async-done(((bf16[1024,2048]{1,0:T(8,128)(2,1)}), bf16[1024,512]{1,0:T(8,128)(2,1)}) %reduce-scatter.2.cloned.1.call-update) | async-done | bytes 1048592 | tf_op jit(solution)/shard_map/reduce_scatter | solution.py:20
  276.7 4.6 %copy.11 = bf16[2048,1024]{1,0:T(8,128)(2,1)} copy(bf16[2048,1024]{1,0:T(8,128)(2,1)} %all-gather.6.cloned.1.call-done) | data formatting | bytes 8388608
  (1 shorter events, 0.0 us)
Async XLA Ops:
  7.2 79.1 %all-gather.8.cloned.1.call-start = ((), (), s32[]{:S(2)}) async-start(), calls=%async_computation.4 | async-start | bytes 4718592 | tf_op jit(solution)/shard_map/all_gather | solution.py:11
  9.3 134.1 %all-gather.4.cloned.1.call-start = ((), (), s32[]{:S(2)}) async-start(), calls=%async_computation.2 | async-start | bytes 5242880 | tf_op jit(solution)/shard_map/all_gather | solution.py:13
  10.1 208.8 %all-gather.6.cloned.1.call-start = ((), (), s32[]{:S(2)}) async-start(), calls=%async_computation.3 | async-start | bytes 4718592 | tf_op jit(solution)/shard_map/all_gather | solution.py:9
  86.2 75.6 %all-to-all-start = ((bf16[4,1024,512]{2,1,0:T(8,128)(2,1)}), bf16[4,1024,512]{2,1,0:T(8,128)(2,1)}, u32[]{:S(2)}, u32[]{:S(2)}) async-start(bf16[4,1024,512]{2,1,0:T(8,128)(2,1)} %bitcast.8), calls=%async_computation | async-start | bytes 8388608 | tf_op jit(solution)/shard_map/all_to_all | solution.py:12
  91.1 185.6 %reduce-scatter.2.cloned.1.call-start = ((), (), s32[]{:S(2)}) async-start(), calls=%async_computation.5 | async-start | bytes 5242880 | tf_op jit(solution)/shard_map/reduce_scatter | solution.py:20
Sparse Core Ops, SparseCore 0:
  10.7 75.5 all-gather.7
  87.8 55.5 all-gather.3
  146.1 72.7 all-gather.5
  233.7 42.9 reduce-scatter.1
where the time goes:
time: 288 us
  waiting for transfers between devices  230 us (80%)
  local copies, waits for them, and re-layouts  17.3 us (6%)
  matrix products  14.7 us (5%)
  between operations  13.8 us (5%)
  other arithmetic  7.31 us (3%)
  starting transfers between devices  5.06 us (2%)
    all_gather x1, waiting for transfers between devices, shards(): gathered = lax.all_gather(down_local, 'fs', axis=0, tiled=True)  73.9 us
    all_gather x1, waiting for transfers between devices, shards(): features = lax.all_gather(tokens, 'tp', axis=1, tiled=True)  52.2 us
    all_gather x1, waiting for transfers between devices, shards(): up_ready = lax.all_gather(up_local, 'fs', axis=0, tiled=True)  50.9 us
    reduce_scatter x1, waiting for transfers between devices, shards(): lax.psum_scatter(partial_value.astype(jnp.bfloat16), 'tp', scatter_dimens...  36.6 us
    all_to_all x1, waiting for transfers between devices, shards(): lax.all_to_all(gathered, 'tp', split_axis=0, concat_axis=1, tiled=True)  15.3 us
    dot_general x1, matrix products, shards(): jnp.dot(hidden, down_ready, preferred_element_type=jnp.float32)  14.7 us
    unnamed x2, local copies, waits for them, and re-layouts  11.1 us
    all_to_all x1, local copies, waits for them, and re-layouts, shards(): lax.all_to_all(gathered, 'tp', split_axis=0, concat_axis=1, tiled=True)  6.21 us
  transfers between devices with their start and end apart: 5, of which 5 were waited for; matrix products, arithmetic and copies ran while one was open for 6% of the time, Pallas kernels for 0%

commit v1 on v0

--- a/solution.py
+++ b/solution.py
@@ -10,7 +10,7 @@
     down_local = down_master.astype(jnp.bfloat16)
     gathered = lax.all_gather(down_local, "fs", axis=0, tiled=True)
     down_ready = lax.all_to_all(gathered, "tp", split_axis=0, concat_axis=1, tiled=True)
-    features = lax.all_gather(tokens, "tp", axis=1, tiled=True)
+    features = jnp.concatenate(lax.all_gather(tokens, "tp"), axis=1)
     values = features.astype(jnp.float32)
     mean_square = jnp.mean(values * values, axis=-1, keepdims=True)
     normed = (values * lax.rsqrt(mean_square + 1e-06)).astype(jnp.bfloat16)

time: 288 us -> 288 us (level)
  waiting for transfers between devices: 230 us -> 207 us
  other arithmetic: 7.31 us -> 20.7 us
  local copies, waits for them, and re-layouts: 17.3 us -> 26.1 us
    all_to_all x1, waiting for transfers between devices: 15.3 us -> 0.01 us  [shards(): lax.all_to_all(gathered, 'tp', split_axis=0, concat_axis=1, tiled=True)]
    convert_element_type x0 -> x2, other arithmetic: none -> 13.3 us  [the longest x1 6.71 us: shards(): normed = (values * lax.rsqrt(mean_square + 1e-06)).astype(jnp.bfloat16)]
    convert_element_type x0 -> x1, local copies, waits for them, and re-layouts: none -> 8.81 us  [shards(): values = features.astype(jnp.float32)]
    all_gather x1, waiting for transfers between devices: 50.9 us -> 43.5 us  [shards(): up_ready = lax.all_gather(up_local, 'fs', axis=0, tiled=True)]
  transfers between devices with their start and end apart: 5 -> 5, of which waited for: 5 -> 4; matrix products, arithmetic and copies ran while one was open for 6% -> 14% of each run, Pallas kernels for 0% -> 0%
where the time goes in v1:
time: 288 us; the launch traced here: 287 us
  waiting for transfers between devices  207 us (72%)
  local copies, waits for them, and re-layouts  26.1 us (9%)
  other arithmetic  20.7 us (7%)
  matrix products  14.4 us (5%)
  between operations  13.8 us (5%)
  starting transfers between devices  5.09 us (2%)
    all_gather x1, waiting for transfers between devices, shards(): gathered = lax.all_gather(down_local, 'fs', axis=0, tiled=True)  73.9 us
    all_gather x1, waiting for transfers between devices, shards(): features = jnp.concatenate(lax.all_gather(tokens, 'tp'), axis=1)  52.2 us
    all_gather x1, waiting for transfers between devices, shards(): up_ready = lax.all_gather(up_local, 'fs', axis=0, tiled=True)  43.5 us
    reduce_scatter x1, waiting for transfers between devices, shards(): lax.psum_scatter(partial_value.astype(jnp.bfloat16), 'tp', scatter_dimens...  36.7 us
    dot_general x1, matrix products, shards(): jnp.dot(hidden, down_ready, preferred_element_type=jnp.float32)  14.4 us
    unnamed x2, local copies, waits for them, and re-layouts  11.1 us
    convert_element_type x1, local copies, waits for them, and re-layouts, shards(): values = features.astype(jnp.float32)  8.81 us
    convert_element_type x1, other arithmetic, shards(): normed = (values * lax.rsqrt(mean_square + 1e-06)).astype(jnp.bfloat16)  6.71 us
  transfers between devices with their start and end apart: 5, of which 4 were waited for; matrix products, arithmetic and copies ran while one was open for 14% of the time, Pallas kernels for 0%

profile of v1, /device:TPU:0, one launch (start us, length us, event | category | flops | bytes accessed | tf_op | source)
XLA Modules:
  0.0 287.0 jit_solution(16237834668280082924)
XLA Ops:
  7.2 0.0 all-gather.7.cloned.1.call-start
  7.2 2.1 convert_element_type.35
  9.3 0.0 all-gather.7.cloned.1.call-update
  9.3 0.0 all-gather.9.cloned.1.call-start
  9.4 0.7 all-gather.9.cloned.1.call-update
  10.1 0.0 all-gather.5.cloned.1.call-start
  10.1 2.2 multiply_convert_fusion.1
  12.3 0.0 all-gather.5.cloned.1.call-update
  12.3 73.9 %all-gather.7.cloned.1.call-done = bf16[4096,512]{1,0:T(8,128)(2,1)} async-done(((bf16[512,512]{1,0:T(8,128)(2,1)}), bf16[4096,512]{1,0:T(8,128)(2,1)}) %all-gather.7.cloned.1.call-update) | async-done | bytes 4194320 | tf_op jit(solution)/shard_map/all_gather | solution.py:11
  86.2 4.9 %all-to-all-start = ((bf16[4,1024,512]{2,1,0:T(8,128)(2,1)}), bf16[4,1024,512]{2,1,0:T(8,128)(2,1)}, u32[]{:S(2)}, u32[]{:S(2)}) async-start(bf16[4,1024,512]{2,1,0:T(8,128)(2,1)} %bitcast.19), calls=%async_computation | async-start | bytes 8388608 | tf_op jit(solution)/shard_map/all_to_all | solution.py:12
  91.2 0.0 reduce-scatter.2.cloned.1.call-start
  91.2 52.2 %all-gather.9.cloned.1.call-done = bf16[4096,512]{1,0:T(8,128)(2,1)} async-done(((bf16[1024,512]{1,0:T(8,128)(2,1)}), bf16[4096,512]{1,0:T(8,128)(2,1)}) %all-gather.9.cloned.1.call-update) | async-done | bytes 4194320 | tf_op jit(solution)/shard_map/all_gather | solution.py:13
  143.4 6.6 %convert_bitcast_fusion = f32[1024,4,512]{2,0,1:T(8,128)} fusion(bf16[4096,512]{1,0:T(8,128)(2,1)} %all-gather.9.cloned.1.call-done), kind=kLoop, calls=%fused_computation.1 | loop fusion | flops 2097152 | bytes 12582912 | tf_op jit(solution)/shard_map/convert_element_type | solution.py:14
  150.0 8.8 %copy.12 = f32[1024,4,512]{0,2,1:T(8,128)} copy(f32[1024,4,512]{2,0,1:T(8,128)} %convert_bitcast_fusion) | data formatting | bytes 16777216 | tf_op jit(solution)/shard_map/convert_element_type | solution.py:14
  158.8 3.1 %fusion = f32[1024]{0:T(1024)S(1)} fusion(bf16[4,1024,512]{2,1,0:T(8,128)(2,1)} %bitcast.16), kind=kLoop, calls=%fused_computation.2 | loop fusion | flops 6290432 | bytes 4198400 | tf_op jit(solution)/shard_map/reduce_sum | solution.py:15
  161.9 6.7 %fusion.1 = bf16[1024,2048]{0,1:T(8,128)(2,1)} fusion(f32[1024,4,512]{0,2,1:T(8,128)} %copy.12, f32[1024]{0:T(1024)S(1)} %add_rsqrt_fusion), kind=kLoop, calls=%fused_computation.4 | loop fusion | flops 4194304 | bytes 12587008 | tf_op jit(solution)/shard_map/convert_element_type | solution.py:16
  168.6 0.0 all-to-all-done
  168.6 6.2 %copy.13 = bf16[4,1024,512]{1,2,0:T(8,128)(2,1)} copy(bf16[4,1024,512]{2,1,0:T(8,128)(2,1)} %all-to-all-done) | data formatting | bytes 8388608 | tf_op jit(solution)/shard_map/all_to_all | solution.py:12
  174.8 43.5 %all-gather.5.cloned.1.call-done = bf16[2048,1024]{1,0:T(8,128)(2,1)} async-done(((bf16[256,1024]{1,0:T(8,128)(2,1)}), bf16[2048,1024]{1,0:T(8,128)(2,1)}) %all-gather.5.cloned.1.call-update) | async-done | bytes 4194320 | tf_op jit(solution)/shard_map/all_gather | solution.py:9
  218.3 14.4 %convolution_convert_fusion = bf16[1024,2048]{1,0:T(8,128)(2,1)} fusion(bf16[1024,2048]{0,1:T(8,128)(2,1)} %bitcast.17, bf16[1024,2048]{0,1:T(8,128)(2,1)} %fusion.1, bf16[2048,1024]{1,0:T(8,128)(2,1)} %all-gather.5.cloned.1.call-done), kind=kOutput, calls=%fused_computation.6 | convolution fusion | flops 8595177472 | bytes 16777216 | tf_op jit(solution)/shard_map/dot_general | solution.py:19
  232.7 0.0 reduce-scatter.2.cloned.1.call-update
  232.7 6.5 %copy.14 = bf16[1024,2048]{1,0:T(8,128)(2,1)} copy(bf16[1024,2048]{0,1:T(8,128)(2,1)} %bitcast.18) | data formatting | bytes 8388608
  239.2 36.7 %reduce-scatter.2.cloned.1.call-done = bf16[1024,512]{1,0:T(8,128)(2,1)} async-done(((bf16[1024,2048]{1,0:T(8,128)(2,1)}), bf16[1024,512]{1,0:T(8,128)(2,1)}) %reduce-scatter.2.cloned.1.call-update) | async-done | bytes 1048592 | tf_op jit(solution)/shard_map/reduce_scatter | solution.py:20
  275.8 4.6 %copy.16 = bf16[2048,1024]{1,0:T(8,128)(2,1)} copy(bf16[2048,1024]{1,0:T(8,128)(2,1)} %all-gather.5.cloned.1.call-done) | data formatting | bytes 8388608
  (1 shorter events, 0.0 us)
Async XLA Ops:
  7.2 79.1 %all-gather.7.cloned.1.call-start = ((), (), s32[]{:S(2)}) async-start(), calls=%async_computation.3 | async-start | bytes 4718592 | tf_op jit(solution)/shard_map/all_gather | solution.py:11
  9.3 134.1 %all-gather.9.cloned.1.call-start = ((), (), s32[]{:S(2)}) async-start(), calls=%async_computation.5 | async-start | bytes 5242880 | tf_op jit(solution)/shard_map/all_gather | solution.py:13
  10.1 208.3 %all-gather.5.cloned.1.call-start = ((), (), s32[]{:S(2)}) async-start(), calls=%async_computation.2 | async-start | bytes 4718592 | tf_op jit(solution)/shard_map/all_gather | solution.py:9
  86.2 82.4 %all-to-all-start = ((bf16[4,1024,512]{2,1,0:T(8,128)(2,1)}), bf16[4,1024,512]{2,1,0:T(8,128)(2,1)}, u32[]{:S(2)}, u32[]{:S(2)}) async-start(bf16[4,1024,512]{2,1,0:T(8,128)(2,1)} %bitcast.19), calls=%async_computation | async-start | bytes 8388608 | tf_op jit(solution)/shard_map/all_to_all | solution.py:12
  91.2 184.7 %reduce-scatter.2.cloned.1.call-start = ((), (), s32[]{:S(2)}) async-start(), calls=%async_computation.4 | async-start | bytes 5242880 | tf_op jit(solution)/shard_map/reduce_scatter | solution.py:20
Sparse Core Ops, SparseCore 0:
  10.7 75.5 all-gather.6
  87.8 55.5 all-gather.8
  145.5 72.7 all-gather.4
  232.9 42.9 reduce-scatter.1
